TPU v7x, 32 devices: a whole 2x2x4 slice. The times are simulated.
32 devices in a mesh: fs: 8 (over z, y), tp: 4 (over x, core).
Axes of the slice: x: 2, y: 2, z: 4, core: 2. Of those that a mesh axis runs over, the one named last changes fastest.
Arguments:
- hidden_in: bfloat16 [512, 4096], P(None, 'tp'), may hold values from -6 to 6
- up_act: bfloat16 [512, 12288], P('tp', 'fs'), may hold values from -6 to 6
- up_val: bfloat16 [512, 12288], P('tp', 'fs'), may hold values from -6 to 6
- cotangent: bfloat16 [512, 4096], P('tp'), may hold values from -6 to 6
- w_act: bfloat16 [4096, 12288], P('tp', 'fs'), may hold values from -0.09375 to 0.09375
- w_val: bfloat16 [4096, 12288], P('tp', 'fs'), may hold values from -0.09375 to 0.09375
- w_down: bfloat16 [12288, 4096], P('fs', 'tp'), may hold values from -0.0546875 to 0.0546875
- conv_act: bfloat16 [3, 12288], P(None, 'fs'), may hold values from -3 to 3
- conv_val: bfloat16 [3, 12288], P(None, 'fs'), may hold values from -3 to 3
- bias_act: bfloat16 [12288], P('fs'), may hold values from -3 to 3
- bias_val: bfloat16 [12288], P('fs'), may hold values from -3 to 3
Outputs:
- grad_input: bfloat16 [512, 4096], P(('tp', 'fs'))
- grad_w_act: float32 [4096, 12288], P('tp', 'fs')
- grad_w_val: float32 [4096, 12288], P('tp', 'fs')
- grad_w_down: float32 [12288, 4096], P('fs', 'tp')
- grad_conv_act: float32 [3, 12288], P(None, 'fs')
- grad_conv_val: float32 [3, 12288], P(None, 'fs')
- grad_bias_act: float32 [12288], P('fs')
- grad_bias_val: float32 [12288], P('fs')
- rows_act: float32 [4096], P('tp')
- rows_val: float32 [4096], P('tp')
- rows_down: float32 [12288], P('fs')
- conv_rows: float32 [2, 3], replicated
All inputs are finite; a program needn't handle non-finite values.
Results may differ from a plain program's by a relative error of at most 0.0057.
Values may be sent and summed in bfloat16 or wider, within the bound.
A program may use at most 128 MiB of HBM per device.

v0:
```python
import jax
import jax.numpy as jnp
from jax import lax
from jax.sharding import PartitionSpec as P


def passed_along(value, axis, by):
    length = lax.axis_size(axis)
    pairs = [(i, i + by) for i in range(length) if 0 <= i + by < length]
    return lax.ppermute(value, axis, pairs)


def contract_last(left, right):
    return lax.dot_general(
        left, right, (((1,), (1,)), ((), ())), preferred_element_type=jnp.float32
    )


def contract_first(left, right):
    return lax.dot_general(
        left, right, (((0,), (0,)), ((), ())), preferred_element_type=jnp.float32
    )


def conv_ahead(extended, taps, bias, length):
    total = jnp.zeros((length, extended.shape[1]), jnp.float32) + bias.astype(jnp.float32)
    for offset in range(taps.shape[0]):
        total = total + taps[offset].astype(jnp.float32) * extended[offset : offset + length]
    return total


def conv_behind(extended, taps, length):
    reach = taps.shape[0] - 1
    total = jnp.zeros((length, extended.shape[1]), jnp.float32)
    for offset in range(taps.shape[0]):
        total = (
            total
            + taps[offset].astype(jnp.float32) * extended[reach - offset : reach - offset + length]
        )
    return total.astype(jnp.bfloat16)


def tap_grads(grad_pre, extended, tap_count):
    length = grad_pre.shape[0]
    rows = [
        jnp.sum(grad_pre * extended[offset : offset + length], axis=0)
        for offset in range(tap_count)
    ]
    return (jnp.stack(rows, 0), jnp.sum(grad_pre, axis=0))


def per_device(
    hidden_in,
    up_act,
    up_val,
    cotangent,
    w_act,
    w_val,
    w_down,
    conv_act,
    conv_val,
    bias_act,
    bias_val,
):
    local_rows = cotangent.shape[0]
    tap_count = conv_act.shape[0]
    reach = tap_count - 1
    tp_count = lax.axis_size("tp")
    fs_count = lax.axis_size("fs")
    down_whole = lax.all_gather(w_down, "tp", axis=1, tiled=True)
    prev_act, prev_val = passed_along(
        (up_act[local_rows - reach :], up_val[local_rows - reach :]), "tp", 1
    )
    ext_act = jnp.concatenate([prev_act, up_act], 0).astype(jnp.float32)
    ext_val = jnp.concatenate([prev_val, up_val], 0).astype(jnp.float32)
    pre_act = conv_ahead(ext_act, conv_act, bias_act, local_rows)
    pre_val = conv_ahead(ext_val, conv_val, bias_val, local_rows)
    gelu_act, gelu_back = jax.vjp(jax.nn.gelu, pre_act)
    mixed = (gelu_act * pre_val).astype(jnp.bfloat16)
    grad_mixed = contract_last(cotangent, down_whole).astype(jnp.bfloat16)
    grad_mixed = lax.optimization_barrier(grad_mixed).astype(jnp.float32)
    grad_pre_act = gelu_back(grad_mixed * pre_val)[0]
    grad_pre_val = grad_mixed * gelu_act
    next_act, next_val = passed_along((grad_pre_act[:reach], grad_pre_val[:reach]), "tp", -1)
    grad_up_act = conv_behind(jnp.concatenate([grad_pre_act, next_act], 0), conv_act, local_rows)
    grad_up_val = conv_behind(jnp.concatenate([grad_pre_val, next_val], 0), conv_val, local_rows)
    taps_act, sums_act = tap_grads(grad_pre_act, ext_act, tap_count)
    taps_val, sums_val = tap_grads(grad_pre_val, ext_val, tap_count)
    all_up_act, all_up_val, all_mixed = (
        lax.all_gather(grad_up_act, "tp", axis=0, tiled=True),
        lax.all_gather(grad_up_val, "tp", axis=0, tiled=True),
        lax.all_gather(mixed, "tp", axis=0, tiled=True),
    )
    cot_columns = lax.all_to_all(cotangent, "tp", split_axis=1, concat_axis=0, tiled=True)
    grad_w_act = contract_first(hidden_in, all_up_act)
    grad_w_val = contract_first(hidden_in, all_up_val)
    grad_w_down = contract_first(all_mixed, cot_columns)
    shard_rows = local_rows // fs_count
    block_rows = tp_count * shard_rows

    def select_rows(gathered):
        shaped = gathered.reshape(tp_count, fs_count, shard_rows, gathered.shape[1])
        return jnp.transpose(shaped, (1, 0, 2, 3)).reshape(
            lax.axis_size("fs") * block_rows, gathered.shape[1]
        )

    summed = lax.psum_scatter(
        contract_last(select_rows(all_up_act), w_act)
        + contract_last(select_rows(all_up_val), w_val),
        "fs",
        scatter_dimension=0,
        tiled=True,
    ).astype(jnp.bfloat16)
    grad_input = lax.all_to_all(summed, "tp", split_axis=0, concat_axis=1, tiled=True)
    down_squares = jnp.sum(grad_w_down * grad_w_down, axis=1)
    taps_act, taps_val, sums_act, sums_val, rows_down = lax.psum(
        (taps_act, taps_val, sums_act, sums_val, down_squares), "tp"
    )
    tap_squares = jnp.stack(
        [jnp.sum(taps_act * taps_act, axis=1), jnp.sum(taps_val * taps_val, axis=1)], 0
    )
    rows_act, rows_val, conv_rows = lax.psum(
        (
            jnp.sum(grad_w_act * grad_w_act, axis=1),
            jnp.sum(grad_w_val * grad_w_val, axis=1),
            tap_squares,
        ),
        "fs",
    )
    return (
        grad_input,
        grad_w_act,
        grad_w_val,
        grad_w_down,
        taps_act,
        taps_val,
        sums_act,
        sums_val,
        rows_act,
        rows_val,
        rows_down,
        conv_rows,
    )


def solution(mesh):
    return jax.shard_map(
        per_device,
        mesh=mesh,
        in_specs=(
            P(None, "tp"),
            P("tp", "fs"),
            P("tp", "fs"),
            P("tp", None),
            P("tp", "fs"),
            P("tp", "fs"),
            P("fs", "tp"),
            P(None, "fs"),
            P(None, "fs"),
            P("fs"),
            P("fs"),
        ),
        out_specs=(
            P(("tp", "fs"), None),
            P("tp", "fs"),
            P("tp", "fs"),
            P("fs", "tp"),
            P(None, "fs"),
            P(None, "fs"),
            P("fs"),
            P("fs"),
            P("tp"),
            P("tp"),
            P("fs"),
            P(),
        ),
        check_vma=False,
    )
```

profile of v0, /device:TPU:0, one launch (start us, length us, event | category | flops | bytes accessed | tf_op | source)
XLA Modules:
  0.0 296.1 jit_solution(9692622403794457745)
XLA Ops:
  7.2 0.0 copy-start
  7.2 0.0 all-gather.5.cloned.1.call-start
  7.2 0.7 all-gather.5.cloned.1.call-update
  7.9 0.0 all-gather.9.cloned.1.call-start
  8.0 0.4 copy-done.10
  8.4 2.4 collective-permute-start.1
  10.8 0.8 slice.74
  11.5 4.5 %collective-permute-start = (bf16[2,1536]{1,0:T(2,128)(2,1)S(1)}, bf16[2,1536]{1,0:T(2,128)(2,1)S(1)}, u32[]{:S(2)}, u32[]{:S(2)}) collective-permute-start(bf16[2,1536]{1,0:T(2,128)(2,1)S(1)} %slice.74), channel_id=1, source_target_pairs={{0,1},{1,2},{2,3},{4,5},{5,6},{6,7},{8,9},{9,10},{10,11},{12,13},{... | collective-permute-start | bytes 18440 | tf_op jit(solution)/shard_map/ppermute | solution.py:10
  16.0 1.5 convert_reduce_fusion.5
  17.5 1.3 convert_element_type.52
  18.8 0.0 collective-permute-done.1
  18.8 1.0 maximum_convert_fusion.1
  19.8 0.0 collective-permute-done
  19.8 2.1 maximum_convert_fusion
  21.9 72.5 %all-gather.5.cloned.1.call-done = bf16[1536,4096]{1,0:T(8,128)(2,1)} async-done(((bf16[1536,1024]{1,0:T(8,128)(2,1)}), bf16[1536,4096]{1,0:T(8,128)(2,1)}) %all-gather.5.cloned.1.call-update) | async-done | bytes 12582928 | tf_op jit(solution)/shard_map/all_gather | solution.py:70
  94.4 9.3 %convolution_convert_fusion = bf16[128,1536]{1,0:T(8,128)(2,1)S(1)} fusion(bf16[128,4096]{1,0:T(8,128)(2,1)} %param.14, bf16[1536,4096]{1,0:T(8,128)(2,1)} %all-gather.5.cloned.1.call-done), kind=kOutput, calls=%fused_computation.5 | convolution fusion | flops 1610809344 | bytes 14024704 | tf_op jit(solution)/shard_map/dot_general | solution.py:14
  103.8 0.0 copy-start.13
  103.8 0.0 copy-start.16
  103.8 0.9 multiply_reduce_fusion.5
  104.7 0.0 copy-start.4
  104.7 1.3 collective-permute-start.3
  106.0 0.1 convert_reduce_fusion.4
  106.1 1.7 collective-permute-done.3
  107.8 2.1 multiply_reduce_fusion.8
  109.9 0.0 all-gather.9.cloned.1.call-update
  109.9 0.0 all-gather.7.cloned.1.call-start
  110.0 0.8 slice.98
  110.8 1.3 collective-permute-start.2
  112.1 3.5 %collective-permute-done.2 = f32[2,1536]{1,0:T(2,128)S(1)} collective-permute-done((f32[2,1536]{1,0:T(2,128)S(1)}, f32[2,1536]{1,0:T(2,128)S(1)}, u32[]{:S(2)}, u32[]{:S(2)}) %collective-permute-start.2) | collective-permute-done | bytes 12320 | tf_op jit(solution)/shard_map/ppermute | solution.py:10
  115.5 3.0 fusion.9
  118.5 0.0 all-gather.7.cloned.1.call-update
  118.5 0.0 all-gather.11.cloned.1.call-start
  118.6 2.5 multiply_convert_fusion
  121.1 0.0 all-gather.11.cloned.1.call-update
  121.1 0.0 reduce-scatter.2.cloned.1.call-start
  121.2 10.4 %all-gather.9.cloned.1.call-done = bf16[512,1536]{1,0:T(8,128)(2,1)} async-done(((bf16[128,1536]{1,0:T(8,128)(2,1)}), bf16[512,1536]{1,0:T(8,128)(2,1)}) %all-gather.9.cloned.1.call-update) | async-done | bytes 1572880 | tf_op jit(solution)/shard_map/all_gather | solution.py:91
  131.5 2.7 copy.34
  134.2 18.6 %all-gather.7.cloned.1.call-done = bf16[512,1536]{1,0:T(8,128)(2,1)} async-done(((bf16[128,1536]{1,0:T(8,128)(2,1)}), bf16[512,1536]{1,0:T(8,128)(2,1)}) %all-gather.7.cloned.1.call-update) | async-done | bytes 1572880 | tf_op jit(solution)/shard_map/all_gather | solution.py:90
  152.8 1.5 copy.33
  154.3 0.0 copy-start.8
  154.3 0.0 copy-start.17
  154.3 1.8 fusion.19
  156.2 0.5 copy-done.17
  156.7 3.2 %convolution_add_fusion = f32[512,1024]{1,0:T(8,128)} fusion(f32[512,1024]{1,0:T(8,128)S(1)} %fusion.19, bf16[512,1536]{1,0:T(8,128)(2,1)S(1)} %bitcast.37, bf16[1024,1536]{1,0:T(8,128)(2,1)S(1)} %copy-done.17), kind=kOutput, calls=%fused_computation.6 | convolution fusion | flops 1611137024 | bytes 8912896 | tf_op jit(solution)/shard_map/dot_general | solution.py:14
  159.8 0.0 reduce-scatter.2.cloned.1.call-update
  159.9 1.3 copy-done.5
  161.1 0.7 copy.36
  161.8 21.8 %all_to_all.38 = bf16[128,4,1024]{0,2,1:T(8,128)(2,1)S(1)} all-to-all(bf16[128,4,1024]{0,2,1:T(8,128)(2,1)S(1)} %bitcast.34), channel_id=1, replica_groups=mesh['fs'=8,'tp'=4] {'tp'}, dimensions={1} | all-to-all | bytes 2097152 | tf_op jit(solution)/shard_map/all_to_all | solution.py:94
  183.6 1.3 copy.37
  185.0 0.3 copy-done.7
  185.4 5.8 %multiply_reduce_fusion.1 = (f32[1024]{0:T(1024)S(1)}, f32[1024,1536]{0,1:T(8,128)}) fusion(bf16[512,1536]{1,0:T(8,128)(2,1)S(1)} %copy-done.7, bf16[512,1024]{1,0:T(8,128)(2,1)} %param.11), kind=kOutput, calls=%fused_computation.1 | convolution fusion | flops 1613757440 | bytes 8916992 | tf_op jit(solution)/shard_map/dot_general | solution.py:20
  191.1 6.7 %copy.39 = f32[1024,1536]{1,0:T(8,128)} copy(f32[1024,1536]{0,1:T(8,128)} %get-tuple-element.80) | data formatting | bytes 12582912
  197.8 6.0 %multiply_reduce_fusion = (f32[1536]{0:T(1024)S(1)}, f32[1536,1024]{0,1:T(8,128)}) fusion(bf16[512,1536]{1,0:T(8,128)(2,1)} %all-gather.11.cloned.1.call-done, bf16[512,1024]{1,0:T(8,128)(2,1)S(1)} %bitcast.39), kind=kOutput, calls=%fused_computation | convolution fusion | flops 1613756928 | bytes 8919040 | tf_op jit(solution)/shard_map/dot_general | solution.py:20
  203.8 6.7 %copy.40 = f32[1536,1024]{1,0:T(8,128)} copy(f32[1536,1024]{0,1:T(8,128)} %get-tuple-element.76) | data formatting | bytes 12582912
  210.5 11.9 %all-reduce.1 = (f32[3,1536]{1,0:T(4,128)S(1)}, f32[3,1536]{1,0:T(4,128)S(1)}, f32[1536]{0:T(1024)}, f32[1536]{0:T(1024)}, f32[1536]{0:T(1024)}) all-reduce(f32[3,1536]{1,0:T(4,128)S(1)} %pad_maximum_fusion.2, f32[3,1536]{1,0:T(4,128)S(1)} %pad_maximum_fusion.3, ...), channel_id=1, replica_groups=mesh['fs'=8,'tp'=4] {'tp'}, use_global_device_ids=true, to_apply=%region_4.0 | all-reduce | flops 13824 | bytes 110592 | tf_op jit(solution)/shard_map/psum | solution.py:116
  222.4 0.2 multiply_reduce_fusion.9
  222.6 28.7 %reduce-scatter.2.cloned.1.call-done = f32[64,1024]{1,0:T(8,128)} async-done(((f32[512,1024]{1,0:T(8,128)}), f32[64,1024]{1,0:T(8,128)}) %reduce-scatter.2.cloned.1.call-update) | async-done | bytes 262160 | tf_op jit(solution)/shard_map/reduce_scatter | solution.py:107
  251.3 1.6 convert_element_type.56
  252.9 3.3 %all-to-all-start = ((bf16[4,16,1024]{2,1,0:T(8,128)(2,1)}), bf16[4,16,1024]{2,1,0:T(8,128)(2,1)S(1)}, u32[]{:S(2)}, u32[]{:S(2)}) async-start(bf16[4,16,1024]{2,1,0:T(8,128)(2,1)} %bitcast.6), calls=%async_computation.1 | async-start | bytes 262144 | tf_op jit(solution)/shard_map/all_to_all | solution.py:114
  256.3 5.7 %multiply_reduce_fusion.2 = (f32[1024]{0:T(1024)S(1)}, f32[1024,1536]{0,1:T(8,128)}) fusion(bf16[512,1536]{1,0:T(8,128)(2,1)S(1)} %copy-done.6, bf16[512,1024]{1,0:T(8,128)(2,1)} %param.11), kind=kOutput, calls=%fused_computation.2 | convolution fusion | flops 1613757440 | bytes 8916992 | tf_op jit(solution)/shard_map/dot_general | solution.py:20
  262.0 6.7 %copy.38 = f32[1024,1536]{1,0:T(8,128)} copy(f32[1024,1536]{0,1:T(8,128)} %get-tuple-element.78) | data formatting | bytes 12582912
  268.7 20.2 %all-reduce = (f32[1024]{0:T(1024)}, f32[1024]{0:T(1024)}, f32[2,3]{1,0:T(2,128)}) all-reduce(f32[1024]{0:T(1024)S(1)} %get-tuple-element.77, f32[1024]{0:T(1024)S(1)} %get-tuple-element.79, f32[2,3]{1,0:T(2,128)S(1)} %pad_maximum_fusion.4), channel_id=1, replica_groups=mesh['fs'=8,'tp'=4] {'fs'}, use_global_device_ids=true, to_apply=%region_14.0 | all-reduce | flops 2054 | bytes 16432 | tf_op jit(solution)/shard_map/psum | solution.py:122
  288.9 0.0 all-to-all-done
  288.9 0.7 copy.41
  (39 shorter events, 0.2 us)
Async XLA Ops:
  7.2 147.1 %copy-start = (bf16[1024,1536]{1,0:T(8,128)(2,1)S(1)}, bf16[1024,1536]{1,0:T(8,128)(2,1)}, u32[]{:S(2)}) copy-start(bf16[1024,1536]{1,0:T(8,128)(2,1)} %param.15) | copy-start | bytes 9437188
  7.2 1.1 copy-start.10
  7.2 87.2 %all-gather.5.cloned.1.call-start = ((), (), s32[]{:S(2)}) async-start(), calls=%async_computation.3 | async-start | bytes 15728640 | tf_op jit(solution)/shard_map/all_gather | solution.py:70
  7.9 123.6 %all-gather.9.cloned.1.call-start = ((), (), s32[]{:S(2)}) async-start(), calls=%async_computation.5 | async-start | bytes 1966080 | tf_op jit(solution)/shard_map/all_gather | solution.py:91
  8.4 10.4 %collective-permute-start.1 = (bf16[2,1536]{1,0:T(2,128)(2,1)S(1)}, bf16[2,1536]{1,0:T(2,128)(2,1)S(1)}, u32[]{:S(2)}, u32[]{:S(2)}) collective-permute-start(bf16[2,1536]{1,0:T(2,128)(2,1)S(1)} %slice.80), channel_id=1, source_target_pairs={{0,1},{1,2},{2,3},{4,5},{5,6},{6,7},{8,9},{9,10},{10,11},{12,13},{... | collective-permute-start | bytes 18440 | tf_op jit(solution)/shard_map/ppermute | solution.py:10
  11.5 8.3 %collective-permute-start = (bf16[2,1536]{1,0:T(2,128)(2,1)S(1)}, bf16[2,1536]{1,0:T(2,128)(2,1)S(1)}, u32[]{:S(2)}, u32[]{:S(2)}) collective-permute-start(bf16[2,1536]{1,0:T(2,128)(2,1)S(1)} %slice.74), channel_id=1, source_target_pairs={{0,1},{1,2},{2,3},{4,5},{5,6},{6,7},{8,9},{9,10},{10,11},{12,13},{... | collective-permute-start | bytes 18440 | tf_op jit(solution)/shard_map/ppermute | solution.py:10
  21.9 81.8 %copy-start.11 = (f32[1536]{0:T(1024)S(1)}, f32[1536]{0:T(1024)}, u32[]{:S(2)}) copy-start(f32[1536]{0:T(1024)} %get-tuple-element.61) | copy-start | bytes 18436
  21.9 81.8 %copy-start.12 = (f32[1536]{0:T(1024)S(1)}, f32[1536]{0:T(1024)}, u32[]{:S(2)}) copy-start(f32[1536]{0:T(1024)} %convert_element_type.52) | copy-start | bytes 18436
  94.4 9.3 %copy-start.2 = (f32[130,1536]{1,0:T(8,128)S(1)}, f32[130,1536]{1,0:T(8,128)}, u32[]{:S(2)}) copy-start(f32[130,1536]{1,0:T(8,128)} %maximum_convert_fusion.1) | copy-start | bytes 2396164
  94.4 9.3 %copy-start.3 = (f32[130,1536]{1,0:T(8,128)S(1)}, f32[130,1536]{1,0:T(8,128)}, u32[]{:S(2)}) copy-start(f32[130,1536]{1,0:T(8,128)} %maximum_convert_fusion) | copy-start | bytes 2396164
  103.8 2.2 copy-start.13
  103.8 2.3 copy-start.16
  104.7 5.2 %copy-start.4 = (f32[128,1536]{1,0:T(8,128)}, f32[128,1536]{1,0:T(8,128)S(1)}, u32[]{:S(2)}) copy-start(f32[128,1536]{1,0:T(8,128)S(1)} %get-tuple-element.71) | copy-start | bytes 2359300
  104.7 3.1 %collective-permute-start.3 = (f32[2,1536]{1,0:T(2,128)S(1)}, f32[2,1536]{1,0:T(2,128)S(1)}, u32[]{:S(2)}, u32[]{:S(2)}) collective-permute-start(f32[2,1536]{1,0:T(2,128)S(1)} %slice.101), channel_id=1, source_target_pairs={{1,0},{2,1},{3,2},{5,4},{6,5},{7,6},{9,8},{10,9},{11,10},{13,12},{... | collective-permute-start | bytes 36872 | tf_op jit(solution)/shard_map/ppermute | solution.py:10
  109.9 42.9 %all-gather.7.cloned.1.call-start = ((), (), s32[]{:S(2)}) async-start(), calls=%async_computation.4 | async-start | bytes 1966080 | tf_op jit(solution)/shard_map/all_gather | solution.py:90
  110.8 4.8 %collective-permute-start.2 = (f32[2,1536]{1,0:T(2,128)S(1)}, f32[2,1536]{1,0:T(2,128)S(1)}, u32[]{:S(2)}, u32[]{:S(2)}) collective-permute-start(f32[2,1536]{1,0:T(2,128)S(1)} %slice.98), channel_id=1, source_target_pairs={{1,0},{2,1},{3,2},{5,4},{6,5},{7,6},{9,8},{10,9},{11,10},{13,12},{... | collective-permute-start | bytes 36872 | tf_op jit(solution)/shard_map/ppermute | solution.py:10
  118.5 79.3 %all-gather.11.cloned.1.call-start = ((), (), s32[]{:S(2)}) async-start(), calls=%async_computation.7 | async-start | bytes 1966080 | tf_op jit(solution)/shard_map/all_gather | solution.py:92
  121.1 130.2 %reduce-scatter.2.cloned.1.call-start = ((), (), s32[]{:S(2)}) async-start(), calls=%async_computation.6 | async-start | bytes 2359296 | tf_op jit(solution)/shard_map/reduce_scatter | solution.py:107
  154.3 1.9 copy-start.8
  154.3 2.4 copy-start.17
  159.8 1.3 copy-start.5
  183.6 1.8 copy-start.7
  191.1 6.7 %copy-start.9 = (bf16[4,128,1024]{2,1,0:T(8,128)(2,1)S(1)}, bf16[4,128,1024]{2,1,0:T(8,128)(2,1)}, u32[]{:S(2)}) copy-start(bf16[4,128,1024]{2,1,0:T(8,128)(2,1)} %copy.37) | copy-start | bytes 3145732
  203.8 52.5 %copy-start.6 = (bf16[512,1536]{1,0:T(8,128)(2,1)S(1)}, bf16[512,1536]{1,0:T(8,128)(2,1)}, u32[]{:S(2)}) copy-start(bf16[512,1536]{1,0:T(8,128)(2,1)} %all-gather.7.cloned.1.call-done) | copy-start | bytes 4718596
  222.4 39.5 %copy-start.14 = (f32[3,1536]{1,0:T(4,128)}, f32[3,1536]{1,0:T(4,128)S(1)}, u32[]{:S(2)}) copy-start(f32[3,1536]{1,0:T(4,128)S(1)} %get-tuple-element.65) | copy-start | bytes 55300
  222.4 39.5 %copy-start.15 = (f32[3,1536]{1,0:T(4,128)}, f32[3,1536]{1,0:T(4,128)S(1)}, u32[]{:S(2)}) copy-start(f32[3,1536]{1,0:T(4,128)S(1)} %get-tuple-element.66) | copy-start | bytes 55300
  252.9 35.9 %all-to-all-start = ((bf16[4,16,1024]{2,1,0:T(8,128)(2,1)}), bf16[4,16,1024]{2,1,0:T(8,128)(2,1)S(1)}, u32[]{:S(2)}, u32[]{:S(2)}) async-start(bf16[4,16,1024]{2,1,0:T(8,128)(2,1)} %bitcast.6), calls=%async_computation.1 | async-start | bytes 262144 | tf_op jit(solution)/shard_map/all_to_all | solution.py:114
  262.0 27.5 %copy-start.1 = (bf16[1024,1536]{1,0:T(8,128)(2,1)S(1)}, bf16[1024,1536]{1,0:T(8,128)(2,1)}, u32[]{:S(2)}) copy-start(bf16[1024,1536]{1,0:T(8,128)(2,1)} %param.15) | copy-start | bytes 9437188
Sparse Core Ops, SparseCore 0:
  9.6 84.7 all-gather.4
  110.0 21.4 all-gather.8
  133.1 19.6 all-gather.6
  154.2 24.6 all-gather.10
  182.2 68.9 reduce-scatter.1
where the time goes:
time: 297 us; the launch traced here: 296 us
  waiting for transfers between devices  136 us (46%)
  blocking collectives  53.9 us (18%)
  matrix products  31.7 us (11%)
  local copies, waits for them, and re-layouts  31 us (10%)
  other arithmetic  16.2 us (5%)
  between operations  14.1 us (5%)
  starting transfers between devices  13 us (4%)
    all_gather x1, waiting for transfers between devices, per_device(): down_whole = lax.all_gather(w_down, 'tp', axis=1, tiled=True)  72.5 us
    reduce_scatter x1, waiting for transfers between devices, per_device(): lax.psum_scatter(contract_last(select_rows(all_up_act), w_act) + contract...  28.7 us
    unnamed x40, local copies, waits for them, and re-layouts  23.3 us
    all_to_all x1, blocking collectives, per_device(): lax.all_to_all(cotangent, 'tp', split_axis=1, concat_axis=0, tiled=True)  21.8 us
    psum x1, blocking collectives, per_device(): lax.psum((jnp.sum(grad_w_act * grad_w_act, axis=1), jnp.sum(grad_w_val *...  20.2 us
    all_gather x1, waiting for transfers between devices, per_device(): lax.all_gather(grad_up_act, 'tp', axis=0, tiled=True)  18.6 us
    dot_general x3, matrix products, contract_first(): lax.dot_general(left, right, (((0,), (0,)), ((), ())), preferred_element_...  17.5 us
    dot_general x3, matrix products, contract_last(): lax.dot_general(left, right, (((1,), (1,)), ((), ())), preferred_element_...  14.3 us
  transfers between devices with their start and end apart: 10, of which 6 were waited for; matrix products, arithmetic and copies ran while one was open for 21% of the time, Pallas kernels for 0%

commit v1 on v0

--- a/solution.py
+++ b/solution.py
@@ -2,6 +2,10 @@
 import jax.numpy as jnp
 from jax import lax
 from jax.sharding import PartitionSpec as P
+
+
+def things_reach(base_x):
+    return jnp.concatenate(lax.all_gather(base_x, "tp"), axis=1)
 
 
 def passed_along(value, axis, by):
@@ -67,7 +71,7 @@
     reach = tap_count - 1
     tp_count = lax.axis_size("tp")
     fs_count = lax.axis_size("fs")
-    down_whole = lax.all_gather(w_down, "tp", axis=1, tiled=True)
+    down_whole = things_reach(w_down)
     prev_act, prev_val = passed_along(
         (up_act[local_rows - reach :], up_val[local_rows - reach :]), "tp", 1
     )

time: 297 us -> 313 us (1.054)
  local copies, waits for them, and re-layouts: 31 us -> 45.2 us
    reshape x0 -> x1, local copies, waits for them, and re-layouts: none -> 16.7 us  [things_reach(): return jnp.concatenate(lax.all_gather(base_x, 'tp'), axis=1)]
    unnamed x40 -> x38, local copies, waits for them, and re-layouts: 23.3 us -> 21.4 us
  transfers between devices with their start and end apart: 10 -> 10, of which waited for: 6 -> 6; matrix products, arithmetic and copies ran while one was open for 21% -> 20% of each run, Pallas kernels for 0% -> 0%
where the time goes in v1:
time: 313 us; the launch traced here: 312 us
  waiting for transfers between devices  138 us (44%)
  blocking collectives  55.5 us (18%)
  local copies, waits for them, and re-layouts  45.2 us (14%)
  matrix products  29.3 us (9%)
  other arithmetic  16.3 us (5%)
  between operations  14.1 us (5%)
  starting transfers between devices  13 us (4%)
    all_gather x1, waiting for transfers between devices, things_reach(): return jnp.concatenate(lax.all_gather(base_x, 'tp'), axis=1)  72.8 us
    reduce_scatter x1, waiting for transfers between devices, per_device(): lax.psum_scatter(contract_last(select_rows(all_up_act), w_act) + contract...  30.7 us
    all_to_all x1, blocking collectives, per_device(): lax.all_to_all(cotangent, 'tp', split_axis=1, concat_axis=0, tiled=True)  23 us
    unnamed x38, local copies, waits for them, and re-layouts  21.4 us
    psum x1, blocking collectives, per_device(): lax.psum((jnp.sum(grad_w_act * grad_w_act, axis=1), jnp.sum(grad_w_val *...  20.1 us
    all_gather x1, waiting for transfers between devices, per_device(): lax.all_gather(grad_up_act, 'tp', axis=0, tiled=True)  18.6 us
    dot_general x3, matrix products, contract_first(): lax.dot_general(left, right, (((0,), (0,)), ((), ())), preferred_element_...  17.5 us
    reshape x1, local copies, waits for them, and re-layouts, things_reach(): return jnp.concatenate(lax.all_gather(base_x, 'tp'), axis=1)  16.7 us
  transfers between devices with their start and end apart: 10, of which 6 were waited for; matrix products, arithmetic and copies ran while one was open for 20% of the time, Pallas kernels for 0%

profile of v1, /device:TPU:0, one launch (start us, length us, event | category | flops | bytes accessed | tf_op | source)
XLA Modules:
  0.0 311.6 jit_solution(2727314219239125867)
XLA Ops:
  7.2 0.0 copy-start
  7.2 0.0 all-gather.12.cloned.1.call-start
  7.2 0.7 all-gather.12.cloned.1.call-update
  7.9 0.0 all-gather.8.cloned.1.call-start
  8.0 0.9 slice.74
  8.9 2.4 collective-permute-start
  11.3 4.5 %collective-permute-start.1 = (bf16[2,1536]{1,0:T(2,128)(2,1)S(1)}, bf16[2,1536]{1,0:T(2,128)(2,1)S(1)}, u32[]{:S(2)}, u32[]{:S(2)}) collective-permute-start(bf16[2,1536]{1,0:T(2,128)(2,1)S(1)} %slice.80), channel_id=1, source_target_pairs={{0,1},{1,2},{2,3},{4,5},{5,6},{6,7},{8,9},{9,10},{10,11},{12,13},{... | collective-permute-start | bytes 18440 | tf_op jit(solution)/shard_map/ppermute | solution.py:14
  15.8 1.5 convert_reduce_fusion.5
  17.3 1.3 convert_element_type.52
  18.6 0.0 collective-permute-done.1
  18.6 1.0 maximum_convert_fusion.1
  19.6 0.0 collective-permute-done
  19.6 2.1 maximum_convert_fusion
  21.6 72.8 %all-gather.12.cloned.1.call-done = bf16[6144,1024]{1,0:T(8,128)(2,1)} async-done(((bf16[1536,1024]{1,0:T(8,128)(2,1)}), bf16[6144,1024]{1,0:T(8,128)(2,1)}) %all-gather.12.cloned.1.call-update) | async-done | bytes 12582928 | tf_op jit(solution)/shard_map/all_gather | solution.py:8
  94.4 16.7 %copy.33 = bf16[1536,4,1024]{0,2,1:T(8,128)(2,1)} copy(bf16[1536,4,1024]{2,0,1:T(8,128)(2,1)} %bitcast.38) | data formatting | bytes 25165824 | tf_op jit(solution)/shard_map/reshape | solution.py:8
  111.1 6.8 %convolution_convert_fusion = bf16[128,1536]{1,0:T(8,128)(2,1)S(1)} fusion(bf16[128,4096]{1,0:T(8,128)(2,1)} %param.14, bf16[1536,4096]{0,1:T(8,128)(2,1)} %bitcast.37), kind=kOutput, calls=%fused_computation.5 | convolution fusion | flops 1610809344 | bytes 14024704 | tf_op jit(solution)/shard_map/dot_general | solution.py:18
  117.9 0.0 copy-start.12
  118.0 0.0 copy-start.15
  118.0 0.9 multiply_reduce_fusion.5
  118.9 0.0 copy-start.4
  118.9 1.3 collective-permute-start.3
  120.2 0.1 convert_reduce_fusion.4
  120.3 1.7 collective-permute-done.3
  122.0 2.1 multiply_reduce_fusion.8
  124.1 0.0 all-gather.8.cloned.1.call-update
  124.1 0.0 all-gather.6.cloned.1.call-start
  124.2 0.8 slice.98
  125.0 1.3 collective-permute-start.2
  126.2 3.5 %collective-permute-done.2 = f32[2,1536]{1,0:T(2,128)S(1)} collective-permute-done((f32[2,1536]{1,0:T(2,128)S(1)}, f32[2,1536]{1,0:T(2,128)S(1)}, u32[]{:S(2)}, u32[]{:S(2)}) %collective-permute-start.2) | collective-permute-done | bytes 12320 | tf_op jit(solution)/shard_map/ppermute | solution.py:14
  129.7 3.0 fusion.9
  132.7 0.0 all-gather.6.cloned.1.call-update
  132.8 0.0 all-gather.10.cloned.1.call-start
  132.8 2.6 multiply_convert_fusion
  135.4 0.0 all-gather.10.cloned.1.call-update
  135.4 0.0 reduce-scatter.2.cloned.1.call-start
  135.5 10.3 %all-gather.8.cloned.1.call-done = bf16[512,1536]{1,0:T(8,128)(2,1)} async-done(((bf16[128,1536]{1,0:T(8,128)(2,1)}), bf16[512,1536]{1,0:T(8,128)(2,1)}) %all-gather.8.cloned.1.call-update) | async-done | bytes 1572880 | tf_op jit(solution)/shard_map/all_gather | solution.py:95
  145.7 2.7 copy.35
  148.4 18.6 %all-gather.6.cloned.1.call-done = bf16[512,1536]{1,0:T(8,128)(2,1)} async-done(((bf16[128,1536]{1,0:T(8,128)(2,1)}), bf16[512,1536]{1,0:T(8,128)(2,1)}) %all-gather.6.cloned.1.call-update) | async-done | bytes 1572880 | tf_op jit(solution)/shard_map/all_gather | solution.py:94
  167.0 1.5 copy.34
  168.5 0.0 copy-done
  168.5 0.0 copy-start.8
  168.5 0.0 copy-start.16
  168.5 1.8 fusion.19
  170.4 0.5 copy-done.16
  170.9 3.2 %convolution_add_fusion = f32[512,1024]{1,0:T(8,128)} fusion(f32[512,1024]{1,0:T(8,128)S(1)} %fusion.19, bf16[512,1536]{1,0:T(8,128)(2,1)S(1)} %bitcast.43, bf16[1024,1536]{1,0:T(8,128)(2,1)S(1)} %copy-done.16), kind=kOutput, calls=%fused_computation.6 | convolution fusion | flops 1611137024 | bytes 8912896 | tf_op jit(solution)/shard_map/dot_general | solution.py:18
  174.0 0.0 reduce-scatter.2.cloned.1.call-update
  174.1 0.7 copy.37
  174.7 23.0 %all_to_all.38 = bf16[128,4,1024]{0,2,1:T(8,128)(2,1)S(1)} all-to-all(bf16[128,4,1024]{0,2,1:T(8,128)(2,1)S(1)} %bitcast.40), channel_id=1, replica_groups=mesh['fs'=8,'tp'=4] {'tp'}, dimensions={1} | all-to-all | bytes 2097152 | tf_op jit(solution)/shard_map/all_to_all | solution.py:98
  197.8 0.5 copy.38
  198.4 0.0 all-gather.10.cloned.1.call-done
  198.5 6.0 %multiply_reduce_fusion = (f32[1536]{0:T(1024)S(1)}, f32[1536,1024]{0,1:T(8,128)}) fusion(bf16[512,1536]{1,0:T(8,128)(2,1)} %all-gather.10.cloned.1.call-done, bf16[512,1024]{1,0:T(8,128)(2,1)S(1)} %bitcast.45), kind=kOutput, calls=%fused_computation | convolution fusion | flops 1613756928 | bytes 8919040 | tf_op jit(solution)/shard_map/dot_general | solution.py:24
  204.4 6.7 %copy.41 = f32[1536,1024]{1,0:T(8,128)} copy(f32[1536,1024]{0,1:T(8,128)} %get-tuple-element.76) | data formatting | bytes 12582912
  211.2 5.8 %multiply_reduce_fusion.1 = (f32[1024]{0:T(1024)S(1)}, f32[1024,1536]{0,1:T(8,128)}) fusion(bf16[512,1536]{1,0:T(8,128)(2,1)S(1)} %copy-done.7, bf16[512,1024]{1,0:T(8,128)(2,1)} %param.11), kind=kOutput, calls=%fused_computation.1 | convolution fusion | flops 1613757440 | bytes 8916992 | tf_op jit(solution)/shard_map/dot_general | solution.py:24
  216.9 6.7 %copy.40 = f32[1024,1536]{1,0:T(8,128)} copy(f32[1024,1536]{0,1:T(8,128)} %get-tuple-element.80) | data formatting | bytes 12582912
  223.7 12.3 %all-reduce.1 = (f32[3,1536]{1,0:T(4,128)S(1)}, f32[3,1536]{1,0:T(4,128)S(1)}, f32[1536]{0:T(1024)}, f32[1536]{0:T(1024)}, f32[1536]{0:T(1024)}) all-reduce(f32[3,1536]{1,0:T(4,128)S(1)} %pad_maximum_fusion.2, f32[3,1536]{1,0:T(4,128)S(1)} %pad_maximum_fusion.3, ...), channel_id=1, replica_groups=mesh['fs'=8,'tp'=4] {'tp'}, use_global_device_ids=true, to_apply=%region_4.0 | all-reduce | flops 13824 | bytes 110592 | tf_op jit(solution)/shard_map/psum | solution.py:120
  236.0 0.2 multiply_reduce_fusion.9
  236.1 30.7 %reduce-scatter.2.cloned.1.call-done = f32[64,1024]{1,0:T(8,128)} async-done(((f32[512,1024]{1,0:T(8,128)}), f32[64,1024]{1,0:T(8,128)}) %reduce-scatter.2.cloned.1.call-update) | async-done | bytes 262160 | tf_op jit(solution)/shard_map/reduce_scatter | solution.py:111
  266.8 1.6 convert_element_type.56
  268.5 3.3 %all-to-all-start = ((bf16[4,16,1024]{2,1,0:T(8,128)(2,1)}), bf16[4,16,1024]{2,1,0:T(8,128)(2,1)S(1)}, u32[]{:S(2)}, u32[]{:S(2)}) async-start(bf16[4,16,1024]{2,1,0:T(8,128)(2,1)} %bitcast.9), calls=%async_computation.1 | async-start | bytes 262144 | tf_op jit(solution)/shard_map/all_to_all | solution.py:118
  271.8 5.7 %multiply_reduce_fusion.2 = (f32[1024]{0:T(1024)S(1)}, f32[1024,1536]{0,1:T(8,128)}) fusion(bf16[512,1536]{1,0:T(8,128)(2,1)S(1)} %copy-done.6, bf16[512,1024]{1,0:T(8,128)(2,1)} %param.11), kind=kOutput, calls=%fused_computation.2 | convolution fusion | flops 1613757440 | bytes 8916992 | tf_op jit(solution)/shard_map/dot_general | solution.py:24
  277.5 6.7 %copy.39 = f32[1024,1536]{1,0:T(8,128)} copy(f32[1024,1536]{0,1:T(8,128)} %get-tuple-element.78) | data formatting | bytes 12582912
  284.3 20.1 %all-reduce = (f32[1024]{0:T(1024)}, f32[1024]{0:T(1024)}, f32[2,3]{1,0:T(2,128)}) all-reduce(f32[1024]{0:T(1024)S(1)} %get-tuple-element.77, f32[1024]{0:T(1024)S(1)} %get-tuple-element.79, f32[2,3]{1,0:T(2,128)S(1)} %pad_maximum_fusion.4), channel_id=1, replica_groups=mesh['fs'=8,'tp'=4] {'fs'}, use_global_device_ids=true, to_apply=%region_14.0 | all-reduce | flops 2054 | bytes 16432 | tf_op jit(solution)/shard_map/psum | solution.py:126
  304.4 0.0 all-to-all-done
  304.4 0.7 copy.42
  (38 shorter events, 0.2 us)
Async XLA Ops:
  7.2 161.3 %copy-start = (bf16[1024,1536]{1,0:T(8,128)(2,1)S(1)}, bf16[1024,1536]{1,0:T(8,128)(2,1)}, u32[]{:S(2)}) copy-start(bf16[1024,1536]{1,0:T(8,128)(2,1)} %param.15) | copy-start | bytes 9437188
  7.2 4.1 %copy-start.9 = (bf16[128,1536]{1,0:T(8,128)(2,1)S(1)}, bf16[128,1536]{1,0:T(8,128)(2,1)}, u32[]{:S(2)}) copy-start(bf16[128,1536]{1,0:T(8,128)(2,1)} %param.12) | copy-start | bytes 1179652
  7.2 87.2 %all-gather.12.cloned.1.call-start = ((), (), s32[]{:S(2)}) async-start(), calls=%async_computation.7 | async-start | bytes 15728640 | tf_op jit(solution)/shard_map/all_gather | solution.py:8
  7.9 137.8 %all-gather.8.cloned.1.call-start = ((), (), s32[]{:S(2)}) async-start(), calls=%async_computation.4 | async-start | bytes 1966080 | tf_op jit(solution)/shard_map/all_gather | solution.py:95
  8.9 10.7 %collective-permute-start = (bf16[2,1536]{1,0:T(2,128)(2,1)S(1)}, bf16[2,1536]{1,0:T(2,128)(2,1)S(1)}, u32[]{:S(2)}, u32[]{:S(2)}) collective-permute-start(bf16[2,1536]{1,0:T(2,128)(2,1)S(1)} %slice.74), channel_id=1, source_target_pairs={{0,1},{1,2},{2,3},{4,5},{5,6},{6,7},{8,9},{9,10},{10,11},{12,13},{... | collective-permute-start | bytes 18440 | tf_op jit(solution)/shard_map/ppermute | solution.py:14
  11.3 7.3 %collective-permute-start.1 = (bf16[2,1536]{1,0:T(2,128)(2,1)S(1)}, bf16[2,1536]{1,0:T(2,128)(2,1)S(1)}, u32[]{:S(2)}, u32[]{:S(2)}) collective-permute-start(bf16[2,1536]{1,0:T(2,128)(2,1)S(1)} %slice.80), channel_id=1, source_target_pairs={{0,1},{1,2},{2,3},{4,5},{5,6},{6,7},{8,9},{9,10},{10,11},{12,13},{... | collective-permute-start | bytes 18440 | tf_op jit(solution)/shard_map/ppermute | solution.py:14
  111.1 6.8 %copy-start.2 = (f32[130,1536]{1,0:T(8,128)S(1)}, f32[130,1536]{1,0:T(8,128)}, u32[]{:S(2)}) copy-start(f32[130,1536]{1,0:T(8,128)} %maximum_convert_fusion.1) | copy-start | bytes 2396164
  111.1 6.8 %copy-start.3 = (f32[130,1536]{1,0:T(8,128)S(1)}, f32[130,1536]{1,0:T(8,128)}, u32[]{:S(2)}) copy-start(f32[130,1536]{1,0:T(8,128)} %maximum_convert_fusion) | copy-start | bytes 2396164
  111.1 6.9 %copy-start.10 = (f32[1536]{0:T(1024)S(1)}, f32[1536]{0:T(1024)}, u32[]{:S(2)}) copy-start(f32[1536]{0:T(1024)} %get-tuple-element.61) | copy-start | bytes 18436
  111.1 6.9 %copy-start.11 = (f32[1536]{0:T(1024)S(1)}, f32[1536]{0:T(1024)}, u32[]{:S(2)}) copy-start(f32[1536]{0:T(1024)} %convert_element_type.52) | copy-start | bytes 18436
  117.9 2.2 copy-start.12
  118.0 2.3 copy-start.15
  118.9 5.2 %copy-start.4 = (f32[128,1536]{1,0:T(8,128)}, f32[128,1536]{1,0:T(8,128)S(1)}, u32[]{:S(2)}) copy-start(f32[128,1536]{1,0:T(8,128)S(1)} %get-tuple-element.71) | copy-start | bytes 2359300
  118.9 3.1 collective-permute-start.3
  124.1 42.9 %all-gather.6.cloned.1.call-start = ((), (), s32[]{:S(2)}) async-start(), calls=%async_computation.3 | async-start | bytes 1966080 | tf_op jit(solution)/shard_map/all_gather | solution.py:94
  125.0 4.8 %collective-permute-start.2 = (f32[2,1536]{1,0:T(2,128)S(1)}, f32[2,1536]{1,0:T(2,128)S(1)}, u32[]{:S(2)}, u32[]{:S(2)}) collective-permute-start(f32[2,1536]{1,0:T(2,128)S(1)} %slice.98), channel_id=1, source_target_pairs={{1,0},{2,1},{3,2},{5,4},{6,5},{7,6},{9,8},{10,9},{11,10},{13,12},{... | collective-permute-start | bytes 36872 | tf_op jit(solution)/shard_map/ppermute | solution.py:14
  132.8 65.7 %all-gather.10.cloned.1.call-start = ((), (), s32[]{:S(2)}) async-start(), calls=%async_computation.6 | async-start | bytes 1966080 | tf_op jit(solution)/shard_map/all_gather | solution.py:96
  135.4 131.4 %reduce-scatter.2.cloned.1.call-start = ((), (), s32[]{:S(2)}) async-start(), calls=%async_computation.5 | async-start | bytes 2359296 | tf_op jit(solution)/shard_map/reduce_scatter | solution.py:111
  168.5 1.9 copy-start.8
  168.5 2.4 copy-start.16
  170.9 3.2 %copy-start.5 = (bf16[128,4096]{1,0:T(8,128)(2,1)S(1)}, bf16[128,4096]{1,0:T(8,128)(2,1)}, u32[]{:S(2)}) copy-start(bf16[128,4096]{1,0:T(8,128)(2,1)} %param.14) | copy-start | bytes 3145732
  204.4 6.7 %copy-start.7 = (bf16[512,1536]{1,0:T(8,128)(2,1)S(1)}, bf16[512,1536]{1,0:T(8,128)(2,1)}, u32[]{:S(2)}) copy-start(bf16[512,1536]{1,0:T(8,128)(2,1)} %all-gather.8.cloned.1.call-done) | copy-start | bytes 4718596
  216.9 54.9 %copy-start.6 = (bf16[512,1536]{1,0:T(8,128)(2,1)S(1)}, bf16[512,1536]{1,0:T(8,128)(2,1)}, u32[]{:S(2)}) copy-start(bf16[512,1536]{1,0:T(8,128)(2,1)} %all-gather.6.cloned.1.call-done) | copy-start | bytes 4718596
  236.0 41.6 %copy-start.13 = (f32[3,1536]{1,0:T(4,128)}, f32[3,1536]{1,0:T(4,128)S(1)}, u32[]{:S(2)}) copy-start(f32[3,1536]{1,0:T(4,128)S(1)} %get-tuple-element.65) | copy-start | bytes 55300
  236.0 41.6 %copy-start.14 = (f32[3,1536]{1,0:T(4,128)}, f32[3,1536]{1,0:T(4,128)S(1)}, u32[]{:S(2)}) copy-start(f32[3,1536]{1,0:T(4,128)S(1)} %get-tuple-element.66) | copy-start | bytes 55300
  268.5 35.9 %all-to-all-start = ((bf16[4,16,1024]{2,1,0:T(8,128)(2,1)}), bf16[4,16,1024]{2,1,0:T(8,128)(2,1)S(1)}, u32[]{:S(2)}, u32[]{:S(2)}) async-start(bf16[4,16,1024]{2,1,0:T(8,128)(2,1)} %bitcast.9), calls=%async_computation.1 | async-start | bytes 262144 | tf_op jit(solution)/shard_map/all_to_all | solution.py:118
  277.5 27.5 %copy-start.1 = (bf16[1024,1536]{1,0:T(8,128)(2,1)S(1)}, bf16[1024,1536]{1,0:T(8,128)(2,1)}, u32[]{:S(2)}) copy-start(bf16[1024,1536]{1,0:T(8,128)(2,1)} %param.15) | copy-start | bytes 9437188
Sparse Core Ops, SparseCore 0:
  9.6 84.7 all-gather.11
  124.2 21.4 all-gather.7
  147.3 19.6 all-gather.5
  168.4 25.8 all-gather.9
  197.7 69.1 reduce-scatter.1
